TPU v7x, 512 devices: a whole 4x8x8 slice. The times are simulated.
512 devices in a mesh: rep: 2 (over z_hi), fs: 32 (over z_lo, y), tp: 8 (over x, core).
Axes of the slice: x: 4, y: 8, z: 8 (z_hi: 2, z_lo: 4; z = z_hi * 4 + z_lo), core: 2. Of those that a mesh axis runs over, the one named last changes fastest.
Arguments:
- states: bfloat16 [24576, 2048], P(('rep', 'fs'), 'tp'), may hold values from -6 to 6
- mix_gain: float32 [2048], replicated, may hold values from 0.1 to 1.9
- w_value: bfloat16 [2048, 2048], P('fs', 'tp'), may hold values from -1 to 1
- w_gate: bfloat16 [2048, 2048], P('fs', 'tp'), may hold values from -0.125 to 0.125
- conv_kernel: float32 [31, 2048], replicated, may hold values from -1 to 1
- chan_gain: float32 [2048], replicated, may hold values from 0.1 to 1.9
- w_mix_out: bfloat16 [2048, 2048], P('fs', 'tp'), may hold values from -0.125 to 0.125
- mlp_gain: float32 [2048], replicated, may hold values from 0.1 to 1.9
- w_up: bfloat16 [2048, 6144], P('fs', 'tp'), may hold values from -0.125 to 0.125
- w_down_t: bfloat16 [2048, 6144], P('fs', 'tp'), may hold values from -0.078125 to 0.078125
Outputs:
- layer_out: bfloat16 [24576, 2048], P(('rep', 'fs'), 'tp')
All inputs are finite; a program needn't handle non-finite values.
Results may differ from a plain program's by a relative error of at most 0.017.
Values may be sent and summed in bfloat16 or wider, within the bound.
A program may use at most 64 MiB of HBM per device.

v0:
```python
import jax
import jax.numpy as jnp
from jax import lax
from jax.sharding import Mesh
from jax.sharding import PartitionSpec as P

D = 2048
KWIDTH = 31
LENGTH = 128
TP = ("tp_0", "tp_1")


EPS = 1e-06


def cut_rows(length, count):
    hop = length // count
    if hop >= 8:
        hop -= hop % 8
    return [hop * k for k in range(1, count)]


def gather_in_order(shard, axes, order):
    pieces = shard
    for k in order:
        pieces = lax.all_gather(pieces, axes[k])
    done = order[::-1]
    back = [done.index(k) for k in range(len(axes))]
    pieces = pieces.transpose(*back, *range(len(axes), pieces.ndim))
    return pieces.reshape(-1, *shard.shape)


def laid_out(pieces, dim):
    pieces = jnp.moveaxis(pieces, 0, dim)
    dims = pieces.shape
    return pieces.reshape(*dims[:dim], dims[dim] * dims[dim + 1], *dims[dim + 2 :])


def gather_at_once(shard, axes, dim):
    split_at = max(range(max(1, shard.ndim - 1)), key=lambda d: shard.shape[d])
    count, outs = (len(axes), [])
    for initial, slab in enumerate(
        jnp.split(shard, cut_rows(shard.shape[split_at], count), axis=split_at)
    ):
        if slab.size:
            order = [(initial - k) % count for k in range(count)]
            outs.append(gather_in_order(slab, axes, order))
    return laid_out(jnp.concatenate(outs, axis=split_at + 1), dim)


def in_one_piece(arrays, axis, dim, along):
    ends, at = ([], 0)
    for a in arrays[:-1]:
        at += a.shape[along]
        ends.append(at)
    both = jnp.concatenate(arrays, axis=along)
    return tuple(jnp.split(lax.all_gather(both, axis, axis=dim, tiled=True), ends, axis=along))


def copy_for_each(shard, axis):
    copies = jnp.broadcast_to(shard, (lax.axis_size(axis), *shard.shape))
    return lax.all_to_all(copies, axis, split_axis=0, concat_axis=0, tiled=True)


def over_copies(shard, axis):
    everything = copy_for_each(shard, axis)
    return jnp.sum(everything, axis=0)


def in_one(arrays, axis):
    ends = [0]
    for a in arrays:
        ends.append(ends[-1] + a.size)
    so_far = over_copies(jnp.concatenate([a.ravel() for a in arrays]), axis)
    return tuple((so_far[b:e].reshape(a.shape) for a, b, e in zip(arrays, ends, ends[1:])))


def in_blocks(shard, dim, count):
    before, after = (shard.shape[:dim], shard.shape[dim + 1 :])
    return jnp.moveaxis(shard.reshape(*before, count, -1, *after), dim, 0)


def summed_on_arrival(shard, axis, dim):
    count = lax.axis_size(axis)
    pieces = lax.all_to_all(in_blocks(shard, dim, count), axis, 0, 0, tiled=True)
    return jnp.sum(pieces.astype(jnp.float32), axis=0)


def collect(shard, axis, dim):
    pieces = copy_for_each(shard, axis)
    return laid_out(pieces, dim)


def rms_norm(rows, gain):
    values = rows.astype(jnp.float32)
    scaled = values * lax.rsqrt(jnp.mean(values * values, axis=-1, keepdims=True) + EPS)
    return (scaled * gain).astype(jnp.bfloat16)


def times_transposed(left, right):
    return lax.dot_general(
        left, right, (((1,), (1,)), ((), ())), preferred_element_type=jnp.float32
    )


def body(
    states, mix_gain, w_value, w_gate, conv_kernel, chan_gain, w_mix_out, mlp_gain, w_up, w_down_t
):
    width = states.shape[1]
    offset = lax.axis_index(TP) * width
    token_rows = states.shape[0]
    whole_rows = gather_at_once(states, TP, 1)
    normed = rms_norm(whole_rows, mix_gain)
    value_full, gate_full, out_full = in_one_piece((w_value, w_gate, w_mix_out), "fs", 0, 1)
    value = jnp.dot(normed, value_full, preferred_element_type=jnp.float32)
    gate = jnp.dot(normed, gate_full, preferred_element_type=jnp.float32)
    gated = value * jax.nn.sigmoid(gate)
    own_kernel = lax.dynamic_slice_in_dim(conv_kernel, offset, width, 1)
    blocks = gated.reshape(token_rows // LENGTH, LENGTH, width)
    padded = jnp.pad(blocks, ((0, 0), (KWIDTH - 1, 0), (0, 0)))
    filtered = jnp.zeros_like(blocks)
    for tap in range(KWIDTH):
        filtered = filtered + own_kernel[tap][None, None, :] * padded[:, tap : tap + LENGTH, :]
    filtered = filtered.reshape(token_rows, width)
    sum_rows, square_rows = in_one(
        (jnp.sum(filtered, axis=-1), jnp.sum(filtered * filtered, axis=-1)), TP
    )
    mean_rows = (sum_rows / D)[:, None]
    variance = (square_rows / D)[:, None] - mean_rows * mean_rows
    own_gain = lax.dynamic_slice_in_dim(chan_gain, offset, width, 0)
    activated = jax.nn.silu((filtered - mean_rows) * lax.rsqrt(variance + EPS) * own_gain).astype(
        jnp.bfloat16
    )
    mixer_terms = times_transposed(activated, out_full)
    mixed = summed_on_arrival(mixer_terms.astype(jnp.bfloat16), TP, 1)
    middle = (states.astype(jnp.float32) + mixed).astype(jnp.bfloat16)
    middle_rows = collect(middle, TP, 1)
    normed_mid = rms_norm(middle_rows, mlp_gain)
    up_full, down_full = in_one_piece((w_up, w_down_t), "fs", 0, 1)
    upward = jnp.dot(normed_mid, up_full, preferred_element_type=jnp.float32)
    hidden = jnp.square(jnp.maximum(upward, 0.0)).astype(jnp.bfloat16)
    fed_terms = times_transposed(hidden, down_full)
    fed = summed_on_arrival(fed_terms.astype(jnp.bfloat16), TP, 1)
    return (middle.astype(jnp.float32) + fed).astype(jnp.bfloat16)


def solution(mesh):
    split = Mesh(
        mesh.devices.reshape(mesh.shape["rep"], mesh.shape["fs"], 4, 2),
        ("rep", "fs", "tp_0", "tp_1"),
    )
    return jax.shard_map(
        body,
        mesh=split,
        in_specs=(
            P(("rep", "fs"), TP),
            P(),
            P("fs", TP),
            P("fs", TP),
            P(),
            P(),
            P("fs", TP),
            P(),
            P("fs", TP),
            P("fs", TP),
        ),
        out_specs=P(("rep", "fs"), TP),
        check_vma=False,
    )
```

profile of v0, /device:TPU:1, one launch (start us, length us, event | category | flops | bytes accessed | tf_op | source)
XLA Modules:
  0.0 372.3 jit_solution(2018714799038196036)
XLA Ops:
  6.5 0.0 all-gather.7.cloned.1.call-start
  6.5 1.4 pad_maximum_fusion.2
  8.0 0.0 all-gather.7.cloned.1.call-update
  8.0 0.0 all-gather.9.cloned.1.call-start
  8.0 1.6 pad_maximum_fusion.1
  9.7 0.0 all-gather.9.cloned.1.call-update
  9.7 1.0 fusion.96
  10.7 10.8 %all-gather = bf16[768,256]{1,0:T(8,128)(2,1)S(1)} all-gather(bf16[192,256]{1,0:T(8,128)(2,1)S(1)} %get-tuple-element.39), channel_id=2, replica_groups=mesh['rep'=2,'fs'=32,'tp_0'=4,'tp_1'=2] {'tp_0'}, dimensions={0}, use_global_device_ids=true | all-gather | bytes 491520 | tf_op jit(solution)/shard_map/all_gather | solution.py:26
  21.5 10.5 %all-gather.1 = bf16[8,192,256]{2,1,0:T(8,128)(2,1)S(1)} all-gather(bf16[4,192,256]{2,1,0:T(8,128)(2,1)S(1)} %bitcast.89), channel_id=3, replica_groups=mesh['rep'=2,'fs'=32,'tp_0'=4,'tp_1'=2] {'tp_1'}, dimensions={0}, use_global_device_ids=true | all-gather | bytes 1179648 | tf_op jit(solution)/shard_map/all_gather | solution.py:26
  32.0 0.1 copy.28
  32.1 0.0 copy-start
  32.1 2.0 all-gather.2
  34.0 11.8 %all-gather.3 = bf16[8,192,256]{2,1,0:T(8,128)(2,1)S(1)} all-gather(bf16[2,192,256]{2,1,0:T(8,128)(2,1)S(1)} %bitcast.90), channel_id=5, replica_groups=mesh['rep'=2,'fs'=32,'tp_0'=4,'tp_1'=2] {'tp_0'}, dimensions={0}, use_global_device_ids=true | all-gather | bytes 983040 | tf_op jit(solution)/shard_map/all_gather | solution.py:26
  45.9 0.0 copy-done
  45.9 0.9 copy-done.1
  46.8 1.9 convert_bitcast_fusion
  48.7 2.4 copy.29
  51.1 1.8 fusion
  52.9 1.1 fusion.95
  54.0 1.3 constant_dynamic-slice_fusion
  55.3 1.5 fusion.8
  56.8 93.8 %all-gather.7.cloned.1.call-done = bf16[2048,768]{1,0:T(8,128)(2,1)} async-done(((bf16[64,768]{1,0:T(8,128)(2,1)}), bf16[2048,768]{1,0:T(8,128)(2,1)}) %all-gather.7.cloned.1.call-update) | async-done | bytes 3145744 | tf_op jit(solution)/shard_map/all_gather | solution.py:57
  150.7 2.3 fusion.23
  153.0 1.8 convolution_multiply_fusion
  154.8 1.6 fusion.93
  156.4 0.6 broadcast_in_dim.4
  157.0 25.9 %all-to-all-start = ((f32[8,1,768]{2,1,0:T(1,128)}), f32[8,1,768]{2,1,0:T(1,128)S(1)}, u32[]{:S(2)}, u32[]{:S(2)}) async-start(f32[8,1,768]{2,1,0:T(1,128)} %broadcast_in_dim.4), calls=%async_computation | async-start | bytes 49152 | tf_op jit(solution)/shard_map/all_to_all | solution.py:62
  183.0 0.8 dynamic_slice.7
  183.7 3.9 %all-to-all-done = f32[8,1,768]{2,1,0:T(1,128)S(1)} async-done(((f32[8,1,768]{2,1,0:T(1,128)}), f32[8,1,768]{2,1,0:T(1,128)S(1)}, u32[]{:S(2)}, u32[]{:S(2)}) %all-to-all-start) | async-done | bytes 24608 | tf_op jit(solution)/shard_map/all_to_all | solution.py:62
  187.7 0.2 multiply_convert_fusion
  187.9 1.8 convolution_convert_fusion
  189.8 0.1 copy.42
  189.9 0.0 copy-start.3
  189.9 23.8 %all_to_all.21 = bf16[8,384,256]{2,1,0:T(8,128)(2,1)S(1)} all-to-all(bf16[8,384,256]{2,1,0:T(8,128)(2,1)S(1)} %bitcast.84), channel_id=1, replica_groups=mesh['rep'=2,'fs'=32,'tp_0'=4,'tp_1'=2] {'tp_0','tp_1'}, dimensions={0} | all-to-all | bytes 3145728 | tf_op jit(solution)/shard_map/all_to_all | solution.py:85
  213.7 0.2 convert_reduce_fusion.1
  214.0 0.1 add_convert_fusion.1
  214.0 0.2 copy.32
  214.2 0.0 copy-start.5
  214.2 0.1 broadcast_in_dim.5
  214.3 24.0 %all_to_all.22 = bf16[8,384,256]{1,2,0:T(8,128)(2,1)S(1)} all-to-all(bf16[8,384,256]{1,2,0:T(8,128)(2,1)S(1)} %broadcast_in_dim.5), channel_id=1, replica_groups=mesh['rep'=2,'fs'=32,'tp_0'=4,'tp_1'=2] {'tp_0','tp_1'}, dimensions={0} | all-to-all | bytes 3145728 | tf_op jit(solution)/shard_map/all_to_all | solution.py:62
  238.4 0.4 multiply_reduce_fusion
  238.8 0.4 fusion.6
  239.2 73.5 %all-gather.9.cloned.1.call-done = bf16[2048,1536]{1,0:T(8,128)(2,1)} async-done(((bf16[64,1536]{1,0:T(8,128)(2,1)}), bf16[2048,1536]{1,0:T(8,128)(2,1)}) %all-gather.9.cloned.1.call-update) | async-done | bytes 6291472 | tf_op jit(solution)/shard_map/all_gather | solution.py:57
  312.7 6.0 %fusion.9 = bf16[384,2048]{1,0:T(8,128)(2,1)S(1)} fusion(bf16[2048,1536]{1,0:T(8,128)(2,1)} %all-gather.9.cloned.1.call-done, bf16[384,2048]{0,1:T(8,128)(2,1)S(1)} %fusion.6), kind=kOutput, calls=%fused_computation.16 | convolution fusion | flops 2417590272 | bytes 9437184 | tf_op jit(solution)/shard_map/dot_general | solution.py:101
  318.7 0.1 copy.41
  318.8 45.7 %all_to_all.23 = bf16[8,384,256]{2,1,0:T(8,128)(2,1)S(1)} all-to-all(bf16[8,384,256]{2,1,0:T(8,128)(2,1)S(1)} %bitcast.85), channel_id=1, replica_groups=mesh['rep'=2,'fs'=32,'tp_0'=4,'tp_1'=2] {'tp_0','tp_1'}, dimensions={0} | all-to-all | bytes 3145728 | tf_op jit(solution)/shard_map/all_to_all | solution.py:85
  364.5 0.2 convert_reduce_fusion
  364.7 0.7 add_convert_fusion
  (12 shorter events, 0.1 us)
Async XLA Ops:
  6.5 144.1 %all-gather.7.cloned.1.call-start = ((), (), s32[]{:S(2)}) async-start(), calls=%async_computation.4 | async-start | bytes 3244032 | tf_op jit(solution)/shard_map/all_gather | solution.py:57
  8.0 304.7 %all-gather.9.cloned.1.call-start = ((), (), s32[]{:S(2)}) async-start(), calls=%async_computation.5 | async-start | bytes 6488064 | tf_op jit(solution)/shard_map/all_gather | solution.py:57
  32.1 13.8 %copy-start = (bf16[4,2,192,256]{3,2,1,0:T(8,128)(2,1)}, bf16[4,2,192,256]{3,2,1,0:T(8,128)(2,1)S(1)}, u32[]{:S(2)}) copy-start(bf16[4,2,192,256]{3,2,1,0:T(8,128)(2,1)S(1)} %copy.28) | copy-start | bytes 2359300
  45.9 0.9 copy-start.1
  48.7 6.6 %copy-start.4 = (f32[2048]{0:T(1024)S(1)}, f32[2048]{0:T(1024)}, u32[]{:S(2)}) copy-start(f32[2048]{0:T(1024)} %param.11) | copy-start | bytes 24580
  56.8 96.2 %copy-start.2 = (bf16[384,2048]{0,1:T(8,128)(2,1)S(1)}, bf16[384,2048]{0,1:T(8,128)(2,1)}, u32[]{:S(2)}) copy-start(bf16[384,2048]{0,1:T(8,128)(2,1)} %fusion.8) | copy-start | bytes 4718596
  157.0 30.6 %all-to-all-start = ((f32[8,1,768]{2,1,0:T(1,128)}), f32[8,1,768]{2,1,0:T(1,128)S(1)}, u32[]{:S(2)}, u32[]{:S(2)}) async-start(f32[8,1,768]{2,1,0:T(1,128)} %broadcast_in_dim.4), calls=%async_computation | async-start | bytes 49152 | tf_op jit(solution)/shard_map/all_to_all | solution.py:62
  189.9 24.1 %copy-start.3 = (bf16[384,256]{1,0:T(8,128)(2,1)S(1)}, bf16[384,256]{1,0:T(8,128)(2,1)}, u32[]{:S(2)}) copy-start(bf16[384,256]{1,0:T(8,128)(2,1)} %param.10) | copy-start | bytes 589828
  214.2 24.6 %copy-start.5 = (f32[2048]{0:T(1024)S(1)}, f32[2048]{0:T(1024)}, u32[]{:S(2)}) copy-start(f32[2048]{0:T(1024)} %param.17) | copy-start | bytes 24580
Sparse Core Ops, SparseCore 0:
  9.4 141.2 all-gather.6
  152.8 159.8 all-gather.8
where the time goes:
time: 373 us; the launch traced here: 372 us
  waiting for transfers between devices  171 us (46%)
  blocking collectives  129 us (35%)
  starting transfers between devices  26 us (7%)
  between operations  13.6 us (4%)
  other arithmetic  12.2 us (3%)
  matrix products  12 us (3%)
  local copies, waits for them, and re-layouts  8.6 us (2%)
    all_gather x2, waiting for transfers between devices, in_one_piece(): lax.all_gather(both, axis, axis=dim, tiled=True)  167 us
    all_to_all x2, blocking collectives, summed_on_arrival(): lax.all_to_all(in_blocks(shard, dim, count), axis, 0, 0, tiled=True)  69.5 us
    all_gather x4, blocking collectives, gather_in_order(): pieces = lax.all_gather(pieces, axes[k])  35.1 us
    all_to_all x1, starting transfers between devices, copy_for_each(): return lax.all_to_all(copies, axis, split_axis=0, concat_axis=0, tiled=True)  25.9 us
    all_to_all x1, blocking collectives, copy_for_each(): return lax.all_to_all(copies, axis, split_axis=0, concat_axis=0, tiled=True)  24 us
    dot_general x2, matrix products, times_transposed(): lax.dot_general(left, right, (((1,), (1,)), ((), ())), preferred_element_...  7.85 us
  transfers between devices with their start and end apart: 3, of which 3 were waited for; matrix products, arithmetic and copies ran while one was open for 6% of the time, Pallas kernels for 0%

commit v1 on v0

v1 whole, which is shorter than its diff:
```python
import functools

import jax
import jax.numpy as jnp
from jax import lax
from jax.experimental import pallas as pl
from jax.experimental.pallas import tpu as pltpu
from jax.sharding import PartitionSpec as P

D = 2048
KWIDTH = 31
LENGTH = 128
SEQS = 3
EPS = 1e-06
F32 = jnp.float32
BF16 = jnp.bfloat16

TENSORS = {"vg": (512, 32), "mx": (256, 32), "up": (768, 48), "dn": (768, 32)}
RANK = {"vg": 0, "mx": 1, "up": 2, "dn": 3}
GROUPS = ((0, 1), (6, 8), (1, 3), (3, 6))
FORWARD_SEQS = (0, 2)

RATE = 46600.0
SIBLING_RATE = 300000.0
HOP = 2.2
SIBLING_HOP = 1.0
WINDOW = 4.0


class Plan:
    def __init__(self, send_sems, recv_sems):
        self.copies, self.tasks = {}, {}
        self.send_sems, self.recv_sems = send_sems, recv_sems

    def copy(self, name, src, dst, device, link, needs=(), rank=0):
        index = len(self.copies)
        size = 2 if src.dtype == BF16 else 4
        for extent in src.shape:
            size *= extent
        descriptor = pltpu.make_async_remote_copy(
            src_ref=src,
            dst_ref=dst,
            send_sem=self.send_sems.at[index],
            recv_sem=self.recv_sems.at[index],
            device_id=device,
            device_id_type=pl.DeviceIdType.MESH,
        )
        self.copies[name] = (descriptor, link, size, frozenset(needs), rank)

    def task(self, name, fn, needs, time, rank):
        self.tasks[name] = (fn, frozenset(needs), time, rank)

    def emit(self):
        now, done, free = 0.0, set(), {}
        arrives, waiting = {}, dict(self.copies)
        tasks = dict(self.tasks)
        while waiting or arrives or tasks:
            for name in sorted(waiting, key=lambda n: waiting[n][4]):
                descriptor, link, size, needs, _ = waiting[name]
                if needs <= done and free.get(link, 0.0) - now < WINDOW:
                    near = link == "d"
                    took = size / (SIBLING_RATE if near else RATE)
                    free[link] = max(free.get(link, 0.0), now) + took
                    arrives[name] = free[link] + (SIBLING_HOP if near else HOP)
                    descriptor.start()
                    del waiting[name]
            here = [n for n in arrives if arrives[n] <= now]
            if here:
                first = min(here, key=lambda n: arrives[n])
                self.copies[first][0].wait_recv()
                del arrives[first]
                done.add(first)
                now += 0.02
                continue
            ready = [n for n in tasks if tasks[n][1] <= done]
            if ready:
                best = min(ready, key=lambda n: tasks[n][3])
                fn, _, time, _ = tasks.pop(best)
                fn()
                done.add(best)
                now += time
                continue
            later = list(arrives.values())
            for name in waiting:
                _, link, _, needs, _ = waiting[name]
                if needs <= done:
                    later.append(free[link] - WINDOW + 0.001)
            now = max(now, min(later)) + 1e-6
        for descriptor, *_ in self.copies.values():
            descriptor.wait_send()
        return now


def kernel(
    states, w_value, w_gate, w_mix, w_up, w_down, conv, chan, mix_gain, mlp_gain, out,
    vg, mx, up, dn, full, taps, chan_own, padded, filtered, stats, stats_in, activated, hidden,
    to_sibling, from_sibling, kept, sent, relay_part, relayed, arrived,
    local_sems, send_sems, recv_sems,
):
    rep, fs, tp = lax.axis_index("rep"), lax.axis_index("fs"), lax.axis_index("tp")
    y, z_lo = lax.rem(fs, 8), fs // 8
    z = rep * 4 + z_lo
    x, core = tp // 2, lax.rem(tp, 2)
    step8, step4 = 1 + 6 * core, 1 + 2 * core

    def y_to(hops):
        return {"fs": z_lo * 8 + lax.rem(y + hops * step8, 8)}

    def z_to(hops):
        there = lax.rem(z + hops * step8, 8)
        return {"rep": there // 4, "fs": lax.rem(there, 4) * 8 + y}

    def x_to(hops):
        return {"tp": lax.rem(x + hops * step4, 4) * 2 + core}

    y_ahead, y_back, z_ahead, z_back = y_to(1), y_to(7), z_to(1), z_to(7)
    x_ahead, x_back = x_to(1), x_to(3)
    sibling = {"tp": tp + 1 - 2 * core}

    own = pl.ds(pl.multiple_of(tp * 256, 256), 256)
    loads = [
        (states, full.at[0, 0, 0]),
        (w_value, vg.at[0, 0, :, 0:256]),
        (w_gate, vg.at[0, 0, :, 256:512]),
        (w_mix, mx.at[0, 0]),
        (w_up, up.at[0, 0]),
        (w_down, dn.at[0, 0]),
        (conv.at[:, own], taps),
        (chan.at[:, own], chan_own),
    ]
    loads = [pltpu.make_async_copy(a, b, local_sems.at[i]) for i, (a, b) in enumerate(loads)]
    for load in loads:
        load.start()

    barrier = pltpu.get_barrier_semaphore()
    peers = [y_ahead, y_back, z_ahead, z_back]
    peers += [{"tp": lax.rem(tp + j, 8)} for j in range(1, 8)]
    for peer in peers:
        pl.semaphore_signal(
            barrier, inc=1, device_id=peer, device_id_type=pl.DeviceIdType.MESH
        )
    for tile in range(2):
        for s in range(SEQS):
            padded[tile, s, 0:32, :] = jnp.zeros((32, 128), F32)
    for load in loads:
        load.wait()
    pl.semaphore_wait(barrier, len(peers))

    plan = Plan(send_sems, recv_sems)

    complete = {}
    for name, ref in (("vg", vg), ("mx", mx), ("up", up), ("dn", dn)):
        cut, rank = TENSORS[name][1], RANK[name] * 10
        before = set(plan.copies)
        low, high = pl.ds(0, cut), pl.ds(cut, 64 - cut)
        for d in range(1, 5):
            needs = [f"{name}yF{d - 1}"] if d > 1 else []
            plan.copy(
                f"{name}yF{d}", ref.at[(9 - d) % 8, 0, low], ref.at[8 - d, 0, low], y_ahead, "yF", needs, rank + 1
            )
        for d in range(1, 4):
            needs = [f"{name}yR{d - 1}"] if d > 1 else []
            plan.copy(
                f"{name}yR{d}", ref.at[d - 1, 0, low], ref.at[d, 0, low], y_back, "yR", needs, rank + 1
            )
        group_needs = (
            [],
            [f"{name}yF1", f"{name}yF2"],
            [f"{name}yR1", f"{name}yR2"],
            [f"{name}yR3", f"{name}yF3", f"{name}yF4"],
        )
        for g, (lo, hi) in enumerate(GROUPS):
            rows = pl.ds(lo, hi - lo)
            plan.copy(
                f"{name}zF{g}", ref.at[rows, 0, low], ref.at[rows, 3, low], z_ahead, "zF", group_needs[g], rank + 2
            )
            plan.copy(
                f"{name}zR{g}", ref.at[rows, 0, low], ref.at[rows, 1, low], z_back, "zR", group_needs[g], rank + 2
            )
            if g in (0, 3):
                plan.copy(
                    f"{name}zX{g}", ref.at[rows, 3, low], ref.at[rows, 2, low], z_ahead, "zF", [f"{name}zF{g}"], rank + 2
                )
            else:
                plan.copy(
                    f"{name}zX{g}", ref.at[rows, 1, low], ref.at[rows, 2, low], z_back, "zR", [f"{name}zR{g}"], rank + 2
                )
        plan.copy(f"{name}bF", ref.at[0, 0, high], ref.at[0, 3, high], z_ahead, "zF", [], rank)
        plan.copy(f"{name}bR", ref.at[0, 0, high], ref.at[0, 1, high], z_back, "zR", [], rank)
        plan.copy(
            f"{name}bX", ref.at[0, 3, high], ref.at[0, 2, high], z_ahead, "zF", [f"{name}bF"], rank
        )
        first = [f"{name}bF", f"{name}bR", f"{name}bX"]
        for d in range(1, 5):
            needs = [f"{name}cF{d - 1}"] if d > 1 else first
            plan.copy(
                f"{name}cF{d}", ref.at[(9 - d) % 8, :, high], ref.at[8 - d, :, high], y_ahead, "yF", needs, rank
            )
        for d in range(1, 4):
            needs = [f"{name}cR{d - 1}"] if d > 1 else first
            plan.copy(
                f"{name}cR{d}", ref.at[d - 1, :, high], ref.at[d, :, high], y_back, "yR", needs, rank
            )
        complete[name] = set(plan.copies) - before

    def shards(ref, block):
        at_z = lax.rem((block // 2 + 4 - z_lo) * step4, 4)
        pieces = []
        for i in range(4):
            at_y = lax.rem((lax.rem(block, 2) * 4 + i + 8 - y) * step8, 8)
            pieces.append(ref[at_y, at_z])
        return jnp.concatenate(pieces, axis=0)

    gathered = {}
    for p in range(2):
        for s in range(SEQS):
            rows = full.at[p]
            needs = [f"mid{s}"] if p else []
            name = f"g{p}{s}"
            mine = rows.at[0, 0, s]
            plan.copy(f"{name}F", mine, rows.at[0, 3, s], x_ahead, "xF", needs, 2 + s)
            plan.copy(f"{name}R", mine, rows.at[0, 1, s], x_back, "xR", needs, 2 + s)
            plan.copy(f"{name}S0", mine, rows.at[1, 0, s], sibling, "d", needs, 2 + s)
            if s in FORWARD_SEQS:
                plan.copy(f"{name}X", rows.at[0, 3, s], rows.at[0, 2, s], x_ahead, "xF", [f"{name}F"], 1 + s)
            else:
                plan.copy(f"{name}X", rows.at[0, 1, s], rows.at[0, 2, s], x_back, "xR", [f"{name}R"], 1 + s)
            plan.copy(f"{name}S3", rows.at[0, 3, s], rows.at[1, 1, s], sibling, "d", [f"{name}F"], 2 + s)
            plan.copy(f"{name}S1", rows.at[0, 1, s], rows.at[1, 3, s], sibling, "d", [f"{name}R"], 2 + s)
            plan.copy(f"{name}S2", rows.at[0, 2, s], rows.at[1, 2, s], sibling, "d", [f"{name}X"], 2 + s)
            gathered[p, s] = [name + k for k in ("F", "R", "S0", "X", "S3", "S1", "S2")]

    def normalised(p, s, gain):
        squares = jnp.zeros((LENGTH, 256), F32)
        for side in range(2):
            for at in range(4):
                values = full[p, side, at, s].astype(F32)
                squares = squares + values * values
        scale = lax.rsqrt(jnp.sum(squares, axis=-1, keepdims=True) / D + EPS)
        blocks = []
        for k in range(8):
            side = lax.rem(core + k, 2)
            at = lax.rem((k // 2 + 4 - x) * step4, 4)
            values = full[p, side, at, s].astype(F32)
            blocks.append((values * scale * gain[0:1, 256 * k : 256 * k + 256]).astype(BF16))
        return blocks

    def product(blocks, ref):
        total = None
        for k in range(8):
            term = jnp.dot(blocks[k], shards(ref, k), preferred_element_type=F32)
            total = term if total is None else total + term
        return total

    def gate_task(s):
        both = product(normalised(0, s, mix_gain), vg)
        gated = both[:, 0:256] / (1.0 + jnp.exp(-both[:, 256:512]))
        padded[0, s, 32:160, :] = gated[:, 0:128]
        padded[1, s, 32:160, :] = gated[:, 128:256]

    def filter_task(s):
        sums, squares = 0.0, 0.0
        for tile in range(2):
            lanes = slice(128 * tile, 128 * tile + 128)
            total = jnp.zeros((LENGTH, 128), F32)
            for k in range(KWIDTH):
                total = total + taps[k : k + 1, lanes] * padded[tile, s, 2 + k : 130 + k, :]
            filtered[s, :, lanes] = total
            sums = sums + total
            squares = squares + total * total
        lane = lax.broadcasted_iota(jnp.int32, (LENGTH, 128), 1)
        table = jnp.where(
            lane == 0,
            jnp.sum(sums, axis=-1, keepdims=True),
            jnp.where(lane == 1, jnp.sum(squares, axis=-1, keepdims=True), 0.0),
        )
        stats[s] = table.T[0:8, :]

    def activate_task(s):
        total = stats[s]
        for j in range(7):
            total = total + stats_in[s, j]
        table = jnp.concatenate([total, jnp.zeros((LENGTH - 8, 128), F32)], axis=0).T
        mean = table[:, 0:1] / D
        variance = table[:, 1:2] / D - mean * mean
        scale = lax.rsqrt(variance + EPS)
        v = (filtered[s] - mean) * scale * chan_own[...]
        activated[s] = (v / (1.0 + jnp.exp(-v))).astype(BF16)

    def term(left, ref, towards, which):
        there = lax.rem(x + towards * step4, 4)
        right = shards(ref, there * 2 + which)
        return lax.dot_general(left, right, (((1,), (1,)), ((), ())), preferred_element_type=F32)

    def sibling_task(p, s, left, ref):
        rows = left[s]
        for m in range(4):
            to_sibling[p, s, (4 - m) % 4] = term(rows, ref, m, 1 - core).astype(BF16)

    def own_task(p, s, left, ref):
        rows = left[s]
        direct, later = (3, 1) if s in FORWARD_SEQS else (1, 3)
        for m in (2, direct, later, 0):
            total = term(rows, ref, m, core) + from_sibling[p, s, m].astype(F32)
            if m == 2:
                sent[p, s, 0] = total.astype(BF16)
            elif m == direct:
                sent[p, s, 1] = total.astype(BF16)
            elif m == later:
                relay_part[p, s] = total
            else:
                kept[p, s] = total

    def relay_task(p, s):
        sent[p, s, 2] = (relay_part[p, s] + relayed[p, s].astype(F32)).astype(BF16)

    def total_of(p, s):
        return kept[p, s] + arrived[p, s, 0].astype(F32) + arrived[p, s, 1].astype(F32)

    def middle_task(s):
        full[1, 0, 0, s] = (full[0, 0, 0, s].astype(F32) + total_of(0, s)).astype(BF16)

    def out_task(s):
        result = full[1, 0, 0, s].astype(F32) + total_of(1, s)
        out[LENGTH * s : LENGTH * s + LENGTH, :] = result.astype(BF16)

    def up_task(s):
        upward = jnp.maximum(product(normalised(1, s, mlp_gain), up), 0.0)
        hidden[s] = (upward * upward).astype(BF16)

    for s in range(SEQS):
        plan.task(f"gate{s}", functools.partial(gate_task, s), complete["vg"] | set(gathered[0, s]), 1.0, 50 + s)
        plan.task(f"filter{s}", functools.partial(filter_task, s), [f"gate{s}"], 1.0, 40 + s)
        names = []
        for j in range(1, 8):
            names.append(f"t{s}{j}")
            plan.copy(
                names[-1], stats.at[s], stats_in.at[s, j - 1], {"tp": lax.rem(tp + j, 8)}, "t", [f"filter{s}"], 0
            )
        plan.task(f"act{s}", functools.partial(activate_task, s), names, 0.5, 35 + s)
    for p, (ref, left, weight) in enumerate(((mx, activated, "mx"), (dn, hidden, "dn"))):
        for s in range(SEQS):
            if p == 1:
                plan.task(
                    f"up{s}", functools.partial(up_task, s), complete["up"] | set(gathered[1, s]), 1.2, 25 + s
                )
            source = f"up{s}" if p else f"act{s}"
            name = f"r{p}{s}"
            time = 1.2 if p else 0.6
            plan.task(
                f"{name}sib", functools.partial(sibling_task, p, s, left, ref), complete[weight] | {source}, time, 20 + s
            )
            plan.copy(f"{name}D", to_sibling.at[p, s], from_sibling.at[p, s], sibling, "d", [f"{name}sib"], 0)
            plan.task(f"{name}own", functools.partial(own_task, p, s, left, ref), [f"{name}D"], time, 15 + s)
            ahead = s in FORWARD_SEQS
            towards, link = (x_ahead, "xF") if ahead else (x_back, "xR")
            other, other_link = (x_back, "xR") if ahead else (x_ahead, "xF")
            plan.copy(f"{name}L", sent.at[p, s, 0], relayed.at[p, s], towards, link, [f"{name}own"], 0)
            plan.copy(f"{name}E", sent.at[p, s, 1], arrived.at[p, s, 0], other, other_link, [f"{name}own"], 1)
            plan.task(f"{name}rel", functools.partial(relay_task, p, s), [f"{name}L", f"{name}own"], 0.1, 5 + s)
            plan.copy(f"{name}M", sent.at[p, s, 2], arrived.at[p, s, 1], towards, link, [f"{name}rel"], 0)
            last = functools.partial(out_task if p else middle_task, s)
            plan.task(f"out{s}" if p else f"mid{s}", last, [f"{name}E", f"{name}M"], 0.2, s)
    plan.emit()


COPIES = 4 * 29 + 2 * SEQS * 7 + SEQS * 7 + 2 * SEQS * 4


def body(states, mix_gain, w_value, w_gate, conv_kernel, chan_gain, w_mix_out, mlp_gain, w_up, w_down_t):
    anywhere = pl.BlockSpec(memory_space=pl.ANY)
    vmem = pl.BlockSpec(memory_space=pltpu.VMEM)
    block = (LENGTH, 256)
    return pl.pallas_call(
        kernel,
        name="layer",
        out_shape=jax.ShapeDtypeStruct((SEQS * LENGTH, 256), BF16),
        in_specs=[anywhere] * 8 + [vmem] * 2,
        out_specs=vmem,
        scratch_shapes=[
            *[pltpu.VMEM((8, 4, 64, TENSORS[name][0]), BF16) for name in ("vg", "mx", "up", "dn")],
            pltpu.VMEM((2, 2, 4, SEQS, *block), BF16),
            pltpu.VMEM((KWIDTH, 256), F32),
            pltpu.VMEM((1, 256), F32),
            pltpu.VMEM((2, SEQS, 160, 128), F32),
            pltpu.VMEM((SEQS, *block), F32),
            pltpu.VMEM((SEQS, 8, 128), F32),
            pltpu.VMEM((SEQS, 7, 8, 128), F32),
            pltpu.VMEM((SEQS, *block), BF16),
            pltpu.VMEM((SEQS, LENGTH, 768), BF16),
            pltpu.VMEM((2, SEQS, 4, *block), BF16),
            pltpu.VMEM((2, SEQS, 4, *block), BF16),
            pltpu.VMEM((2, SEQS, *block), F32),
            pltpu.VMEM((2, SEQS, 3, *block), BF16),
            pltpu.VMEM((2, SEQS, *block), F32),
            pltpu.VMEM((2, SEQS, *block), BF16),
            pltpu.VMEM((2, SEQS, 2, *block), BF16),
            pltpu.SemaphoreType.DMA((8,)),
            pltpu.SemaphoreType.DMA((COPIES,)),
            pltpu.SemaphoreType.DMA((COPIES,)),
        ],
        compiler_params=pltpu.CompilerParams(
            collective_id=0, has_side_effects=True, vmem_limit_bytes=48 * 1024 * 1024
        ),
    )(
        states.reshape(SEQS, *block), w_value, w_gate, w_mix_out, w_up, w_down_t, conv_kernel,
        chan_gain.reshape(1, D), mix_gain.reshape(1, D), mlp_gain.reshape(1, D),
    )


def solution(mesh):
    return jax.shard_map(
        body,
        mesh=mesh,
        in_specs=(
            P(("rep", "fs"), "tp"),
            P(),
            P("fs", "tp"),
            P("fs", "tp"),
            P(),
            P(),
            P("fs", "tp"),
            P(),
            P("fs", "tp"),
            P("fs", "tp"),
        ),
        out_specs=P(("rep", "fs"), "tp"),
        check_vma=False,
    )
```

time: 373 us -> 119 us (0.32)
  the two profiles are of different devices: /device:TPU:1 before, /device:TPU:16 now
where the time goes in v1:
time: 119 us; the launch traced here: 118 us
  Pallas kernels  109 us (92%)
  local copies, waits for them, and re-layouts  8.7 us (7%)
    pallas_call x1, Pallas kernels, body(): pl.pallas_call(kernel, name='layer', out_shape=jax.ShapeDtypeStruct((SEQS...  109 us
    unnamed x21, local copies, waits for them, and re-layouts  8.7 us

profile of v1, /device:TPU:16, one launch (start us, length us, event | category | flops | bytes accessed | tf_op | source)
XLA Modules:
  0.0 118.0 jit_solution(6166971349167934380)
XLA Ops:
  0.0 0.0 copy-start
  0.0 0.9 copy-done
  1.0 0.0 copy-start.1
  1.0 0.9 copy-done.1
  1.9 0.0 copy-start.2
  1.9 0.9 copy-done.2
  2.8 0.0 copy-start.3
  2.8 0.9 copy-done.3
  3.7 0.0 copy-start.4
  3.7 0.8 copy-done.4
  4.4 0.0 copy-start.5
  4.4 0.8 copy-done.5
  5.2 0.0 copy-start.6
  5.2 0.8 copy-done.6
  5.9 0.0 copy-start.7
  5.9 0.7 copy-done.7
  6.6 0.0 copy-start.8
  6.6 0.7 copy-done.8
  7.3 0.0 copy-start.9
  7.3 0.7 copy-done.9
  8.0 109.3 %layer.1 = bf16[384,256]{1,0:T(8,128)(2,1)S(1)} custom-call(bf16[3,128,256]{2,1,0:T(8,128)(2,1)S(1)} %bitcast.4, bf16[64,256]{1,0:T(8,128)(2,1)S(1)} %copy-done.4, bf16[64,256]{1,0:T(8,128)(2,1)S(1)} %copy-done.5, bf16[64,256]{1,0:T(8,128)(2,1)S(1)} %copy-done.6, bf16[64,768]{1,0:T(8,128)(2,1)S(1)} %copy-done.2, bf16[64,768]{1,0:T(8,128)(2,1)S(1)} %copy-done.3, ...), custom_call_target="tpu_custom_call" | custom-call | tf_op jit(solution)/shard_map/layer/pallas_call | solution.py:374
  117.3 0.7 copy.12
Async XLA Ops:
  0.0 0.9 copy-start
  1.0 0.9 copy-start.1
  1.9 0.9 copy-start.2
  2.8 0.9 copy-start.3
  3.7 0.8 copy-start.4
  4.4 0.8 copy-start.5
  5.2 0.8 copy-start.6
  5.9 0.7 copy-start.7
  6.6 0.7 copy-start.8
  7.3 0.7 copy-start.9

commit v2 on v1

v2 whole, which is shorter than its diff:
```python
import functools

import jax
import jax.numpy as jnp
from jax import lax
from jax.experimental import pallas as pl
from jax.experimental.pallas import tpu as pltpu
from jax.sharding import PartitionSpec as P

D = 2048
KWIDTH = 31
LENGTH = 128
SEQS = 3
EPS = 1e-06
F32 = jnp.float32
BF16 = jnp.bfloat16

EIGHT = ((0, 1), (7, 8), (1, 2), (6, 7), (2, 3), (5, 6), (3, 4), (4, 5))
FOUR = ((0, 1), (6, 8), (1, 3), (3, 6))
TENSORS = {
    "vg": (512, 32, EIGHT, (0, 2, 4, 6), (0, 1, 2, 3, 4)),
    "mx": (256, 32, FOUR, (0, 3), (0, 2, 4)),
    "up": (768, 48, EIGHT, (0, 2, 4, 6), (0, 2, 4)),
    "dn": (768, 32, FOUR, (0, 3), (0, 1, 2, 3, 4)),
}

RATE = 46600.0
SIBLING_RATE = 300000.0
HOP = 3.2
SIBLING_HOP = 1.0
WINDOW = 1.0


class Plan:
    def __init__(self, send_sems, recv_sems):
        self.copies, self.tasks = {}, {}
        self.send_sems, self.recv_sems = send_sems, recv_sems

    def copy(self, name, src, dst, device, links, needs=()):
        index = len(self.copies)
        size = 2 if src.dtype == BF16 else 4
        for extent in src.shape:
            size *= extent
        descriptor = pltpu.make_async_remote_copy(
            src_ref=src,
            dst_ref=dst,
            send_sem=self.send_sems.at[index],
            recv_sem=self.recv_sems.at[index],
            device_id=device,
            device_id_type=pl.DeviceIdType.MESH,
        )
        took, hop = (size / SIBLING_RATE, SIBLING_HOP) if links == ("d",) else (size / RATE, HOP)
        self.copies[name] = (descriptor, links, took, hop, frozenset(needs))

    def task(self, name, fn, needs, time):
        self.tasks[name] = (fn, frozenset(needs), time)

    def tails(self):
        own = {n: took + hop for n, (_, _, took, hop, _) in self.copies.items()}
        own.update({n: time for n, (_, _, time) in self.tasks.items()})
        users = {n: [] for n in own}
        for table in (self.copies, self.tasks):
            for n, entry in table.items():
                for need in entry[-1] if table is self.copies else entry[1]:
                    users[need].append(n)
        tails = {}

        def tail(n):
            if n not in tails:
                tails[n] = own[n] + max((tail(u) for u in users[n]), default=0.0)
            return tails[n]

        for n in own:
            tail(n)
        return tails

    def emit(self):
        now, done, free = 0.0, set(), {}
        tails = self.tails()
        arrives, tasks = {}, dict(self.tasks)
        order = sorted(self.copies, key=lambda n: -tails[n])
        waiting = {n: self.copies[n] for n in order}
        while waiting or arrives or tasks:
            later = []
            for name in list(waiting):
                descriptor, links, took, hop, needs = waiting[name]
                if not needs <= done:
                    continue
                busy = max(free.get(link, 0.0) for link in links)
                if busy - now < WINDOW:
                    for link in links:
                        free[link] = max(free.get(link, 0.0), now) + took
                    arrives[name] = max(free[link] for link in links) + hop
                    descriptor.start()
                    del waiting[name]
                else:
                    later.append(busy - WINDOW + 0.001)
            here = [n for n in arrives if arrives[n] <= now]
            if here:
                first = min(here, key=lambda n: arrives[n])
                self.copies[first][0].wait_recv()
                del arrives[first]
                done.add(first)
                now += 0.02
                continue
            ready = [n for n in tasks if tasks[n][1] <= done]
            if ready:
                best = max(ready, key=lambda n: tails[n])
                fn, _, time = tasks.pop(best)
                fn()
                done.add(best)
                now += time
                continue
            now = max(now, min(later + list(arrives.values()))) + 1e-6
        for descriptor, *_ in self.copies.values():
            descriptor.wait_send()
        return now


def kernel(
    states, w_value, w_gate, w_mix, w_up, w_down, conv, chan, mix_hbm, mlp_hbm, out,
    vg, mx, up, dn, full, taps, chan_own, padded, filtered, stats, stats_in, activated, hidden,
    to_sibling, from_sibling, kept, sent, arrived, mix_gain, mlp_gain,
    local_sems, send_sems, recv_sems,
):
    rep, fs, tp = lax.axis_index("rep"), lax.axis_index("fs"), lax.axis_index("tp")
    y, z_lo = lax.rem(fs, 8), fs // 8
    z = rep * 4 + z_lo
    x, core = tp // 2, lax.rem(tp, 2)
    step8, step4 = 1 + 6 * core, 1 + 2 * core

    def y_to(hops):
        return {"fs": z_lo * 8 + lax.rem(y + hops * step8, 8)}

    def z_to(hops):
        there = lax.rem(z + hops * step8, 8)
        return {"rep": there // 4, "fs": lax.rem(there, 4) * 8 + y}

    def x_to(hops):
        return {"tp": lax.rem(x + hops * step4, 4) * 2 + core}

    y_ahead, y_back, z_ahead, z_back = y_to(1), y_to(7), z_to(1), z_to(7)
    x_ahead, x_across, x_back = x_to(1), x_to(2), x_to(3)
    sibling = {"tp": tp + 1 - 2 * core}

    own = pl.ds(pl.multiple_of(tp * 256, 256), 256)
    loads = [
        (states, full.at[0, 0, 0]),
        (w_value, vg.at[0, 0, :, 0:256]),
        (w_gate, vg.at[0, 0, :, 256:512]),
        (w_mix, mx.at[0, 0]),
        (w_up, up.at[0, 0]),
        (w_down, dn.at[0, 0]),
        (conv.at[:, own], taps),
        (chan.at[:, own], chan_own),
        (mix_hbm, mix_gain),
        (mlp_hbm, mlp_gain),
    ]
    loads = [pltpu.make_async_copy(a, b, local_sems.at[i]) for i, (a, b) in enumerate(loads)]
    for load in loads:
        load.start()

    barrier = pltpu.get_barrier_semaphore()
    peers = [y_ahead, y_back, z_ahead, z_back]
    peers += [{"tp": lax.rem(tp + j, 8)} for j in range(1, 8)]
    for peer in peers:
        pl.semaphore_signal(
            barrier, inc=1, device_id=peer, device_id_type=pl.DeviceIdType.MESH
        )
    for tile in range(2):
        for s in range(SEQS):
            padded[tile, s, 0:32, :] = jnp.zeros((32, 128), F32)
    for load in loads:
        load.wait()
    pl.semaphore_wait(barrier, len(peers))

    plan = Plan(send_sems, recv_sems)

    complete = {}
    for name, ref in (("vg", vg), ("mx", mx), ("up", up), ("dn", dn)):
        _, cut, groups, forward, cuts = TENSORS[name]
        before = set(plan.copies)
        low, high = pl.ds(0, cut), pl.ds(cut, 64 - cut)
        for d in range(1, 5):
            needs = [f"{name}y{9 - d}"] if d > 1 else []
            plan.copy(f"{name}y{8 - d}", ref.at[(9 - d) % 8, 0, low], ref.at[8 - d, 0, low], y_ahead, ("yF",), needs)
        for d in range(1, 4):
            needs = [f"{name}y{d - 1}"] if d > 1 else []
            plan.copy(f"{name}y{d}", ref.at[d - 1, 0, low], ref.at[d, 0, low], y_back, ("yR",), needs)
        for g, (lo, hi) in enumerate(groups):
            rows = pl.ds(lo, hi - lo)
            needs = [f"{name}y{m}" for m in range(lo, hi) if m]
            plan.copy(f"{name}zF{g}", ref.at[rows, 0, low], ref.at[rows, 3, low], z_ahead, ("zF",), needs)
            plan.copy(f"{name}zR{g}", ref.at[rows, 0, low], ref.at[rows, 1, low], z_back, ("zR",), needs)
            if g in forward:
                plan.copy(f"{name}zX{g}", ref.at[rows, 3, low], ref.at[rows, 2, low], z_ahead, ("zF",), [f"{name}zF{g}"])
            else:
                plan.copy(f"{name}zX{g}", ref.at[rows, 1, low], ref.at[rows, 2, low], z_back, ("zR",), [f"{name}zR{g}"])
        plan.copy(f"{name}b3", ref.at[0, 0, high], ref.at[0, 3, high], z_ahead, ("zF",))
        plan.copy(f"{name}b1", ref.at[0, 0, high], ref.at[0, 1, high], z_back, ("zR",))
        plan.copy(f"{name}b2", ref.at[0, 3, high], ref.at[0, 2, high], z_ahead, ("zF",), [f"{name}b3"])
        for i, (lo, hi) in enumerate(zip(cuts, cuts[1:])):
            at_z = pl.ds(lo, hi - lo)
            first = [f"{name}b{m}" for m in range(lo, hi) if m]
            for d in range(1, 5):
                needs = [f"{name}c{i}{9 - d}"] if d > 1 else first
                plan.copy(
                    f"{name}c{i}{8 - d}", ref.at[(9 - d) % 8, at_z, high], ref.at[8 - d, at_z, high], y_ahead, ("yF",), needs
                )
            for d in range(1, 4):
                needs = [f"{name}c{i}{d - 1}"] if d > 1 else first
                plan.copy(
                    f"{name}c{i}{d}", ref.at[d - 1, at_z, high], ref.at[d, at_z, high], y_back, ("yR",), needs
                )
        complete[name] = set(plan.copies) - before

    def shards(ref, block):
        at_z = lax.rem((block // 2 + 4 - z_lo) * step4, 4)
        pieces = []
        for i in range(4):
            at_y = lax.rem((lax.rem(block, 2) * 4 + i + 8 - y) * step8, 8)
            pieces.append(ref[at_y, at_z])
        return jnp.concatenate(pieces, axis=0)

    gathered = {}
    for p in range(2):
        for s in range(SEQS):
            rows = full.at[p]
            needs = [f"mid{s}"] if p else []
            name = f"g{p}{s}"
            mine = rows.at[0, 0, s]
            plan.copy(f"{name}3", mine, rows.at[0, 3, s], x_ahead, ("xF",), needs)
            plan.copy(f"{name}1", mine, rows.at[0, 1, s], x_back, ("xR",), needs)
            plan.copy(f"{name}2", mine, rows.at[0, 2, s], x_across, ("xF", "xR"), needs)
            plan.copy(f"{name}S0", mine, rows.at[1, 0, s], sibling, ("d",), needs)
            for m in (1, 2, 3):
                plan.copy(f"{name}S{m}", rows.at[0, m, s], rows.at[1, 4 - m, s], sibling, ("d",), [f"{name}{m}"])
            gathered[p, s] = [name + k for k in ("3", "1", "2", "S0", "S1", "S2", "S3")]

    def normalised(p, s, gain):
        squares = jnp.zeros((LENGTH, 256), F32)
        for side in range(2):
            for at in range(4):
                values = full[p, side, at, s].astype(F32)
                squares = squares + values * values
        scale = lax.rsqrt(jnp.sum(squares, axis=-1, keepdims=True) / D + EPS)
        blocks = []
        for k in range(8):
            side = lax.rem(core + k, 2)
            at = lax.rem((k // 2 + 4 - x) * step4, 4)
            values = full[p, side, at, s].astype(F32)
            blocks.append((values * scale * gain[0:1, 256 * k : 256 * k + 256]).astype(BF16))
        return blocks

    def product(blocks, ref):
        total = None
        for k in range(8):
            term = jnp.dot(blocks[k], shards(ref, k), preferred_element_type=F32)
            total = term if total is None else total + term
        return total

    def gate_task(s):
        both = product(normalised(0, s, mix_gain), vg)
        gated = both[:, 0:256] / (1.0 + jnp.exp(-both[:, 256:512]))
        padded[0, s, 32:160, :] = gated[:, 0:128]
        padded[1, s, 32:160, :] = gated[:, 128:256]

    def filter_task(s):
        sums, squares = 0.0, 0.0
        for tile in range(2):
            lanes = slice(128 * tile, 128 * tile + 128)
            total = jnp.zeros((LENGTH, 128), F32)
            for k in range(KWIDTH):
                total = total + taps[k : k + 1, lanes] * padded[tile, s, 2 + k : 130 + k, :]
            filtered[s, :, lanes] = total
            sums = sums + total
            squares = squares + total * total
        lane = lax.broadcasted_iota(jnp.int32, (LENGTH, 128), 1)
        table = jnp.where(
            lane == 0,
            jnp.sum(sums, axis=-1, keepdims=True),
            jnp.where(lane == 1, jnp.sum(squares, axis=-1, keepdims=True), 0.0),
        )
        stats[s] = table.T[0:8, :]

    def activate_task(s):
        total = stats[s]
        for j in range(7):
            total = total + stats_in[s, j]
        table = jnp.concatenate([total, jnp.zeros((LENGTH - 8, 128), F32)], axis=0).T
        mean = table[:, 0:1] / D
        variance = table[:, 1:2] / D - mean * mean
        scale = lax.rsqrt(variance + EPS)
        v = (filtered[s] - mean) * scale * chan_own[...]
        activated[s] = (v / (1.0 + jnp.exp(-v))).astype(BF16)

    def term(left, ref, towards, which):
        there = lax.rem(x + towards * step4, 4)
        right = shards(ref, there * 2 + which)
        return lax.dot_general(left, right, (((1,), (1,)), ((), ())), preferred_element_type=F32)

    def sibling_task(p, s, left, ref):
        rows = left[s]
        for m in range(4):
            to_sibling[p, s, (4 - m) % 4] = term(rows, ref, m, 1 - core).astype(BF16)

    def own_task(p, s, left, ref):
        rows = left[s]
        for m in (2, 1, 3, 0):
            total = term(rows, ref, m, core) + from_sibling[p, s, m].astype(F32)
            if m:
                sent[p, s, m - 1] = total.astype(BF16)
            else:
                kept[p, s] = total

    def total_of(p, s):
        total = kept[p, s]
        for m in range(3):
            total = total + arrived[p, s, m].astype(F32)
        return total

    def middle_task(s):
        full[1, 0, 0, s] = (full[0, 0, 0, s].astype(F32) + total_of(0, s)).astype(BF16)

    def out_task(s):
        result = full[1, 0, 0, s].astype(F32) + total_of(1, s)
        out[LENGTH * s : LENGTH * s + LENGTH, :] = result.astype(BF16)

    def up_task(s):
        upward = jnp.maximum(product(normalised(1, s, mlp_gain), up), 0.0)
        hidden[s] = (upward * upward).astype(BF16)

    for s in range(SEQS):
        plan.task(f"gate{s}", functools.partial(gate_task, s), complete["vg"] | set(gathered[0, s]), 0.4)
        plan.task(f"filter{s}", functools.partial(filter_task, s), [f"gate{s}"], 0.6)
        names = []
        for j in range(1, 8):
            names.append(f"t{s}{j}")
            peer = {"tp": lax.rem(tp + j, 8)}
            plan.copy(names[-1], stats.at[s], stats_in.at[s, j - 1], peer, ("t",), [f"filter{s}"])
        plan.task(f"act{s}", functools.partial(activate_task, s), names, 0.3)
    for p, (ref, left, weight) in enumerate(((mx, activated, "mx"), (dn, hidden, "dn"))):
        for s in range(SEQS):
            if p == 1:
                plan.task(f"up{s}", functools.partial(up_task, s), complete["up"] | set(gathered[1, s]), 0.5)
            source = f"up{s}" if p else f"act{s}"
            name = f"r{p}{s}"
            time = 0.5 if p else 0.25
            plan.task(f"{name}sib", functools.partial(sibling_task, p, s, left, ref), complete[weight] | {source}, time)
            plan.copy(f"{name}D", to_sibling.at[p, s], from_sibling.at[p, s], sibling, ("d",), [f"{name}sib"])
            plan.task(f"{name}own", functools.partial(own_task, p, s, left, ref), [f"{name}D"], time)
            routes = ((x_ahead, ("xF",)), (x_across, ("xF", "xR")), (x_back, ("xR",)))
            for m, (peer, links) in enumerate(routes):
                plan.copy(f"{name}{m}", sent.at[p, s, m], arrived.at[p, s, m], peer, links, [f"{name}own"])
            last = functools.partial(out_task if p else middle_task, s)
            plan.task(f"out{s}" if p else f"mid{s}", last, [f"{name}{m}" for m in range(3)], 0.2)
    plan.emit()


COPIES = sum(7 + 3 * len(groups) + 3 + 7 * (len(cuts) - 1) for _, _, groups, _, cuts in TENSORS.values())
COPIES += 2 * SEQS * 7 + SEQS * 7 + 2 * SEQS * 4


def body(states, mix_gain, w_value, w_gate, conv_kernel, chan_gain, w_mix_out, mlp_gain, w_up, w_down_t):
    anywhere = pl.BlockSpec(memory_space=pltpu.HBM)
    vmem = pl.BlockSpec(memory_space=pltpu.VMEM)
    block = (LENGTH, 256)
    return pl.pallas_call(
        kernel,
        name="layer",
        out_shape=jax.ShapeDtypeStruct((SEQS * LENGTH, 256), BF16),
        in_specs=[anywhere] * 10,
        out_specs=vmem,
        scratch_shapes=[
            *[pltpu.VMEM((8, 4, 64, TENSORS[name][0]), BF16) for name in ("vg", "mx", "up", "dn")],
            pltpu.VMEM((2, 2, 4, SEQS, *block), BF16),
            pltpu.VMEM((KWIDTH, 256), F32),
            pltpu.VMEM((1, 256), F32),
            pltpu.VMEM((2, SEQS, 160, 128), F32),
            pltpu.VMEM((SEQS, *block), F32),
            pltpu.VMEM((SEQS, 8, 128), F32),
            pltpu.VMEM((SEQS, 7, 8, 128), F32),
            pltpu.VMEM((SEQS, *block), BF16),
            pltpu.VMEM((SEQS, LENGTH, 768), BF16),
            pltpu.VMEM((2, SEQS, 4, *block), BF16),
            pltpu.VMEM((2, SEQS, 4, *block), BF16),
            pltpu.VMEM((2, SEQS, *block), F32),
            pltpu.VMEM((2, SEQS, 3, *block), BF16),
            pltpu.VMEM((2, SEQS, 3, *block), BF16),
            pltpu.VMEM((1, D), F32),
            pltpu.VMEM((1, D), F32),
            pltpu.SemaphoreType.DMA((10,)),
            pltpu.SemaphoreType.DMA((COPIES,)),
            pltpu.SemaphoreType.DMA((COPIES,)),
        ],
        compiler_params=pltpu.CompilerParams(
            collective_id=0, has_side_effects=True, vmem_limit_bytes=67043328
        ),
    )(
        states.reshape(SEQS, *block), w_value, w_gate, w_mix_out, w_up, w_down_t, conv_kernel,
        chan_gain.reshape(1, D), mix_gain.reshape(1, D), mlp_gain.reshape(1, D),
    )


def solution(mesh):
    return jax.shard_map(
        body,
        mesh=mesh,
        in_specs=(
            P(("rep", "fs"), "tp"),
            P(),
            P("fs", "tp"),
            P("fs", "tp"),
            P(),
            P(),
            P("fs", "tp"),
            P(),
            P("fs", "tp"),
            P("fs", "tp"),
        ),
        out_specs=P(("rep", "fs"), "tp"),
        check_vma=False,
    )
```

time: 119 us -> 94.7 us (0.80)
  the two profiles are of different devices: /device:TPU:16 before, /device:TPU:1 now
where the time goes in v2:
time: 94.7 us; the launch traced here: 94.5 us
  Pallas kernels  92.9 us (98%)
  local copies, waits for them, and re-layouts  1.62 us (2%)
    pallas_call x1, Pallas kernels, body(): pl.pallas_call(kernel, name='layer', out_shape=jax.ShapeDtypeStruct((SEQS...  92.9 us

profile of v2, /device:TPU:1, one launch (start us, length us, event | category | flops | bytes accessed | tf_op | source)
XLA Modules:
  0.0 94.5 jit_solution(3904096441546315832)
XLA Ops:
  0.0 92.9 %layer.1 = bf16[384,256]{1,0:T(8,128)(2,1)} custom-call(bf16[3,128,256]{2,1,0:T(8,128)(2,1)} %bitcast.4, bf16[64,256]{1,0:T(8,128)(2,1)} %w_value.1, bf16[64,256]{1,0:T(8,128)(2,1)} %w_gate.1, bf16[64,256]{1,0:T(8,128)(2,1)} %w_mix.1, bf16[64,768]{1,0:T(8,128)(2,1)} %w_up.1, bf16[64,768]{1,0:T(8,128)(2,1)} %w_down.1, f32[31,2048]{1,0:T(8,128)} %conv.1, ...), custom_call_target="tpu_custom_call" | custom-call | tf_op jit(solution)/shard_map/layer/pallas_call | solution.py:368
  92.9 1.6 %copy.12 = bf16[384,256]{1,0:T(8,128)(2,1)} copy(bf16[384,256]{1,0:T(8,128)(2,1)} %layer.1) | data formatting | bytes 393216

commit v3 on v2

v3 whole, which is shorter than its diff:
```python
import functools

import jax
import jax.numpy as jnp
from jax import lax
from jax.experimental import pallas as pl
from jax.experimental.pallas import tpu as pltpu
from jax.sharding import PartitionSpec as P

D = 2048
KWIDTH = 31
LENGTH = 128
SEQS = 3
EPS = 1e-06
F32 = jnp.float32
BF16 = jnp.bfloat16

EIGHT = ((0, 1), (7, 8), (1, 2), (6, 7), (2, 3), (5, 6), (3, 4), (4, 5))
FOUR = ((0, 1), (6, 8), (1, 3), (3, 6))


class Way:
    def __init__(self, rows, cut, groups, relay, y, c, far, direct, cuts, bias):
        self.low, self.high = rows
        self.cut, self.groups, self.relay = cut, groups, relay
        self.y, self.c, self.far, self.direct, self.cuts, self.bias = y, c, far, direct, cuts, bias


COLUMNS = {"vg": 512, "mx": 256, "up": 768, "dn": 768}
WAYS = {
    "vg": Way((0, 64), 32, EIGHT, "FRRFFRRF", "ring", "ring", "FFFRRR", True, (0, 1, 2, 3, 4), 2.0),
    "mx": Way((0, 64), 40, FOUR, "FRRF", "ring", "ring", "FFFRRR", True, (0, 2, 4), 2.0),
    "up": Way((0, 64), 48, EIGHT, "FRRFFRRF", "ring", "ring", "FRRFRF", False, (0, 2, 4), 0.0),
    "dn": Way((0, 32), 16, FOUR, "FRRF", "ring", "ring", "FFRFRF", False, (0, 4), 2.0),
    "dm": Way((32, 64), 16, FOUR, "FRRF", "ring", "ring", "FRRFFF", False, (0, 2, 4), -2.0),
}
X_GATHER = ('RRD', 'DRD')
X_SUM = ('RDD', 'DRF')

RATE = 46600.0
SIBLING_RATE = 300000.0
HOP = 3.2
FURTHER_HOP = 0.5
SIBLING_HOP = 1.0
PER_COPY = 0.08
SEND_SLACK = 3.0
WINDOW = 0.3


OPPOSITE = {"y1": "y7", "y7": "y1", "y2": "y6", "y6": "y2", "z1": "z7", "z7": "z1", "x1": "x3", "x3": "x1", "x2": "x2", "d": "d"}


class Plan:
    def __init__(self, send_sems, recv_sems):
        self.copies, self.tasks, self.bias = {}, {}, {}
        self.send_sems, self.recv_sems = send_sems, recv_sems

    def copy(self, name, src, dst, device, links, needs=(), hops=1, along=1, bias=0.0):
        size = 2 if src.dtype == BF16 else 4
        for extent in src.shape:
            size *= extent
        if links == ("d",):
            took, hop = size / SIBLING_RATE, SIBLING_HOP
        else:
            took, hop = size * along / RATE, HOP + FURTHER_HOP * (hops - 1)
        self.copies[name] = ((src, dst, *device), links, took + PER_COPY, hop, frozenset(needs))
        self.bias[name] = bias

    def task(self, name, fn, needs, time):
        self.tasks[name] = (fn, frozenset(needs), time)

    def tails(self):
        own = {n: took + hop for n, (_, _, took, hop, _) in self.copies.items()}
        own.update({n: time for n, (_, _, time) in self.tasks.items()})
        users = {n: [] for n in own}
        for table in (self.copies, self.tasks):
            for n, entry in table.items():
                for need in entry[-1] if table is self.copies else entry[1]:
                    users[need].append(n)
        tails = {}

        def tail(n):
            if n not in tails:
                tails[n] = own[n] + max((tail(u) for u in users[n]), default=0.0)
            return tails[n]

        for n in own:
            tail(n)
        return tails

    def emit(self):
        now, step, done, free = 0.0, 0, set(), {}
        tails = self.tails()
        arrives, tasks = {}, dict(self.tasks)
        order = sorted(self.copies, key=lambda n: -tails[n] - self.bias[n])
        waiting = {n: self.copies[n] for n in order}
        started, started_at, heard, sends, receives, n_sends = {}, {}, {}, [], [], 0
        while waiting or arrives or tasks:
            later = []
            for name in list(waiting):
                (src, dst, where, device), links, took, hop, needs = waiting[name]
                if not needs <= done:
                    continue
                busy = max(free.get(link, 0.0) for link in links)
                if busy - now < WINDOW:
                    for link in links:
                        free[link] = max(free.get(link, 0.0), now) + took
                    left = max(free[link] for link in links)
                    arrives[name] = left + hop
                    if sends and sends[0][0] + SEND_SLACK < now:
                        _, send, last = sends.pop(0)
                        last.wait_send()
                    else:
                        send, n_sends = n_sends, n_sends + 1
                    known = heard.get(OPPOSITE.get(where), -1)
                    receive = next((r for r, at in enumerate(receives) if at < known), len(receives))
                    receives[receive : receive + 1] = [1 << 30]
                    step += 1
                    started_at[name] = step
                    descriptor = pltpu.make_async_remote_copy(
                        src_ref=src,
                        dst_ref=dst,
                        send_sem=self.send_sems.at[send],
                        recv_sem=self.recv_sems.at[receive],
                        device_id=device,
                        device_id_type=pl.DeviceIdType.MESH,
                    )
                    descriptor.start()
                    started[name] = descriptor, where, receive
                    sends.append((left, send, descriptor))
                    sends.sort(key=lambda entry: entry[:2])
                    del waiting[name]
                else:
                    later.append(busy - WINDOW + 0.001)
            here = [n for n in arrives if arrives[n] <= now]
            if here:
                first = min(here, key=lambda n: arrives[n])
                descriptor, where, receive = started.pop(first)
                descriptor.wait_recv()
                step += 1
                receives[receive] = step
                heard[where] = max(heard.get(where, -1), started_at[first])
                del arrives[first]
                done.add(first)
                now += 0.02
                continue
            ready = [n for n in tasks if tasks[n][1] <= done]
            if ready:
                best = max(ready, key=lambda n: tails[n])
                fn, _, time = tasks.pop(best)
                fn()
                done.add(best)
                now += time
                continue
            now = max(now, min(later + list(arrives.values()))) + 1e-6
        for _, _, descriptor in sends:
            descriptor.wait_send()
        assert n_sends <= SEND_SEMS and len(receives) <= RECEIVE_SEMS, (n_sends, len(receives))
        return now


def kernel(
    states, w_value, w_gate, w_mix, w_up, w_down, conv, chan, mix_hbm, mlp_hbm, out,
    vg, mx, up, dn, full, taps, chan_own, padded, filtered, stats, stats_in, activated, hidden,
    mix_gain, mlp_gain, local_sems, send_sems, recv_sems, *buffers,
):
    rep, fs, tp = lax.axis_index("rep"), lax.axis_index("fs"), lax.axis_index("tp")
    y, z_lo = lax.rem(fs, 8), fs // 8
    z = rep * 4 + z_lo
    x, core = tp // 2, lax.rem(tp, 2)
    step8, step4 = 1 + 6 * core, 1 + 2 * core

    def y_to(hops):
        return f"y{hops}", {"fs": z_lo * 8 + lax.rem(y + hops * step8, 8)}

    def z_to(hops):
        there = lax.rem(z + hops * step8, 8)
        return f"z{hops}", {"rep": there // 4, "fs": lax.rem(there, 4) * 8 + y}

    def x_to(hops):
        return f"x{hops}", {"tp": lax.rem(x + hops * step4, 4) * 2 + core}

    y_ahead, y_back, z_ahead, z_back, z_across = y_to(1), y_to(7), z_to(1), z_to(7), z_to(2)
    x_ahead, x_across, x_back = x_to(1), x_to(2), x_to(3)
    sibling = "d", {"tp": tp + 1 - 2 * core}

    own = pl.ds(pl.multiple_of(tp * 256, 256), 256)
    loads = [
        (states, full.at[0, 0, 0]),
        (w_value, vg.at[0, 0, :, 0:256]),
        (w_gate, vg.at[0, 0, :, 256:512]),
        (w_mix, mx.at[0, 0]),
        (w_up, up.at[0, 0]),
        (w_down, dn.at[0, 0]),
        (conv.at[:, own], taps),
        (chan.at[:, own], chan_own),
        (mix_hbm, mix_gain),
        (mlp_hbm, mlp_gain),
    ]
    loads = [pltpu.make_async_copy(a, b, local_sems.at[i]) for i, (a, b) in enumerate(loads)]
    for load in loads:
        load.start()

    barrier = pltpu.get_barrier_semaphore()
    peers = [y_ahead, y_back, z_ahead, z_back]
    if any(way.y != "ring" or way.c != "ring" for way in WAYS.values()):
        peers += [y_to(2), y_to(6)]
    if any(way.direct or "D" in way.relay for way in WAYS.values()):
        peers += [z_across, z_to(6)]
    peers += [("tp", {"tp": lax.rem(tp + j, 8)}) for j in range(1, 8)]
    for _, peer in peers:
        pl.semaphore_signal(
            barrier, inc=1, device_id=peer, device_id_type=pl.DeviceIdType.MESH
        )
    for tile in range(2):
        for s in range(SEQS):
            padded[tile, s, 0:32, :] = jnp.zeros((32, 128), F32)
    for load in loads:
        load.wait()
    pl.semaphore_wait(barrier, len(peers))

    plan = Plan(send_sems, recv_sems)
    wide, narrow = buffers[:7], buffers[7:]

    def along_y(name, block, how, first, far, bias):
        steps = {"F": [(8 - d, (9 - d) % 8) for d in range(1, 4)], "R": [(d, d - 1) for d in range(1, 4)]}
        if how == "ring":
            steps[far].append((4, 5) if far == "F" else (4, 3))
        for way, (link, near, over) in {"F": ("yF", y_ahead, y_to(2)), "R": ("yR", y_back, y_to(6))}.items():
            for m, before in steps[way]:
                if how == "two" and m in (2, 6):
                    plan.copy(f"{name}{m}", block(0), block(m), over, (link,), first, 2, 2, bias)
                else:
                    needs = [f"{name}{before}"] if before else first
                    plan.copy(f"{name}{m}", block(before), block(m), near, (link,), needs, bias=bias)
            if how != "ring" and way == far:
                m = 6 if far == "F" else 2
                plan.copy(f"{name}4", block(m), block(4), over, (link,), [f"{name}{m}"], 2, 2, bias)

    complete = {}
    for name, way in WAYS.items():
        ref = {"vg": vg, "mx": mx, "up": up}.get(name, dn)
        before = set(plan.copies)
        bias = way.bias
        low = pl.ds(way.low, way.cut)
        high = pl.ds(way.low + way.cut, way.high - way.low - way.cut)
        along_y(f"{name}y", lambda m, ref=ref, low=low: ref.at[m, 0, low], way.y, [], way.far[0], bias)
        for g, (lo, hi) in enumerate(way.groups):
            block = [ref.at[pl.ds(lo, hi - lo), m, low] for m in range(4)]
            needs = [f"{name}y{m}" for m in range(lo, hi) if m]
            plan.copy(f"{name}zF{g}", block[0], block[3], z_ahead, ("zF",), needs, bias=bias)
            plan.copy(f"{name}zR{g}", block[0], block[1], z_back, ("zR",), needs, bias=bias)
            if way.relay[g] == "F":
                plan.copy(f"{name}zX{g}", block[3], block[2], z_ahead, ("zF",), [f"{name}zF{g}"], bias=bias)
            elif way.relay[g] == "R":
                plan.copy(f"{name}zX{g}", block[1], block[2], z_back, ("zR",), [f"{name}zR{g}"], bias=bias)
            else:
                plan.copy(f"{name}zX{g}", block[0], block[2], z_across, ("zF", "zR"), needs, 2, bias=bias)
        block = [ref.at[0, m, high] for m in range(4)]
        plan.copy(f"{name}b3", block[0], block[3], z_ahead, ("zF",), bias=bias)
        plan.copy(f"{name}b1", block[0], block[1], z_back, ("zR",), bias=bias)
        if way.direct:
            plan.copy(f"{name}b2", block[0], block[2], z_across, ("zF", "zR"), (), 2, bias=bias)
        elif way.far[1] == "F":
            plan.copy(f"{name}b2", block[3], block[2], z_ahead, ("zF",), [f"{name}b3"], bias=bias)
        else:
            plan.copy(f"{name}b2", block[1], block[2], z_back, ("zR",), [f"{name}b1"], bias=bias)
        for i, (lo, hi) in enumerate(zip(way.cuts, way.cuts[1:])):
            at_z = pl.ds(lo, hi - lo)
            first = [f"{name}b{m}" for m in range(lo, hi) if m]
            along_y(
                f"{name}c{i}", lambda m, ref=ref, at_z=at_z, high=high: ref.at[m, at_z, high], way.c, first, way.far[2 + i], bias
            )
        complete[name] = set(plan.copies) - before

    def shards(ref, block, lo=0, hi=64):
        at_z = lax.rem((block // 2 + 4 - z_lo) * step4, 4)
        pieces = []
        for i in range(4):
            at_y = lax.rem((lax.rem(block, 2) * 4 + i + 8 - y) * step8, 8)
            pieces.append(ref[at_y, at_z, lo:hi])
        return jnp.concatenate(pieces, axis=0)

    gathered = {}
    for p in range(2):
        for s in range(SEQS):
            rows = full.at[p]
            needs = [f"mid{s}"] if p else []
            name = f"g{p}{s}"
            mine = rows.at[0, 0, s]
            plan.copy(f"{name}3", mine, rows.at[0, 3, s], x_ahead, ("xF",), needs)
            plan.copy(f"{name}1", mine, rows.at[0, 1, s], x_back, ("xR",), needs)
            if X_GATHER[p][s] == "D":
                plan.copy(f"{name}2", mine, rows.at[0, 2, s], x_across, ("xF", "xR"), needs, 2)
            elif X_GATHER[p][s] == "F":
                plan.copy(f"{name}2", rows.at[0, 3, s], rows.at[0, 2, s], x_ahead, ("xF",), [f"{name}3"])
            else:
                plan.copy(f"{name}2", rows.at[0, 1, s], rows.at[0, 2, s], x_back, ("xR",), [f"{name}1"])
            plan.copy(f"{name}S0", mine, rows.at[1, 0, s], sibling, ("d",), needs)
            for m in (1, 2, 3):
                plan.copy(f"{name}S{m}", rows.at[0, m, s], rows.at[1, 4 - m, s], sibling, ("d",), [f"{name}{m}"])
            gathered[p, s] = [name + k for k in ("3", "1", "2", "S0", "S1", "S2", "S3")]

    def normalised(p, s, gain):
        squares = jnp.zeros((LENGTH, 256), F32)
        for side in range(2):
            for at in range(4):
                values = full[p, side, at, s].astype(F32)
                squares = squares + values * values
        scale = lax.rsqrt(jnp.sum(squares, axis=-1, keepdims=True) / D + EPS)
        blocks = []
        for k in range(8):
            side = lax.rem(core + k, 2)
            at = lax.rem((k // 2 + 4 - x) * step4, 4)
            values = full[p, side, at, s].astype(F32)
            blocks.append((values * scale * gain[0:1, 256 * k : 256 * k + 256]).astype(BF16))
        return blocks

    def product(blocks, ref):
        total = None
        for k in range(8):
            term = jnp.dot(blocks[k], shards(ref, k), preferred_element_type=F32)
            total = term if total is None else total + term
        return total

    def gate_task(s):
        both = product(normalised(0, s, mix_gain), vg)
        gated = both[:, 0:256] / (1.0 + jnp.exp(-both[:, 256:512]))
        padded[0, s, 32:160, :] = gated[:, 0:128]
        padded[1, s, 32:160, :] = gated[:, 128:256]

    def filter_task(s):
        sums, squares = 0.0, 0.0
        for tile in range(2):
            lanes = slice(128 * tile, 128 * tile + 128)
            total = jnp.zeros((LENGTH, 128), F32)
            for k in range(KWIDTH):
                total = total + taps[k : k + 1, lanes] * padded[tile, s, 2 + k : 130 + k, :]
            filtered[s, :, lanes] = total
            sums = sums + total
            squares = squares + total * total
        lane = lax.broadcasted_iota(jnp.int32, (LENGTH, 128), 1)
        table = jnp.where(
            lane == 0,
            jnp.sum(sums, axis=-1, keepdims=True),
            jnp.where(lane == 1, jnp.sum(squares, axis=-1, keepdims=True), 0.0),
        )
        stats[s] = table.T[0:8, :]

    def activate_task(s):
        total = stats[s]
        for j in range(7):
            total = total + stats_in[s, j]
        table = jnp.concatenate([total, jnp.zeros((LENGTH - 8, 128), F32)], axis=0).T
        mean = table[:, 0:1] / D
        variance = table[:, 1:2] / D - mean * mean
        scale = lax.rsqrt(variance + EPS)
        v = (filtered[s] - mean) * scale * chan_own[...]
        activated[s] = (v / (1.0 + jnp.exp(-v))).astype(BF16)

    class Sums:
        def __init__(self, name, p, s, left, ref, lo, hi, how, buffers):
            self.name, self.s, self.left, self.ref, self.lo, self.hi, self.how = name, s, left, ref, lo, hi, how
            self.to_sibling, self.from_sibling, self.kept, self.sent, self.relay_part, self.relayed, self.arrived = [
                buffer.at[p, s] for buffer in buffers
            ]
            self.width = 4 * (hi - lo)
            self.direct, self.later = {"F": (3, 1), "R": (1, 3), "D": (0, 0)}[how]

        def terms(self, which):
            rows = self.left[self.s]
            at_once = 256 // self.width
            for start in range(0, 4, at_once):
                right = []
                for m in range(start, start + at_once):
                    there = lax.rem(x + m * step4, 4)
                    right.append(shards(self.ref, there * 2 + which, self.lo, self.hi))
                right = right[0] if at_once == 1 else jnp.concatenate(right, axis=0)
                both = lax.dot_general(rows, right, (((1,), (1,)), ((), ())), preferred_element_type=F32)
                for i in range(at_once):
                    yield start + i, both[:, self.width * i : self.width * (i + 1)]

        def sibling_task(self):
            for m, term in self.terms(1 - core):
                self.to_sibling[(4 - m) % 4] = term.astype(BF16)

        def own_task(self):
            for m, term in self.terms(core):
                total = term + self.from_sibling[m].astype(F32)
                if m == 0:
                    self.kept[...] = total
                elif m == self.later:
                    self.relay_part[...] = total
                else:
                    self.sent[m - 1] = total.astype(BF16)

        def relay_task(self):
            self.sent[self.later - 1] = (self.relay_part[...] + self.relayed[...].astype(F32)).astype(BF16)

        def plan(self, needs, time):
            name = self.name
            plan.task(f"{name}sib", self.sibling_task, needs, time)
            plan.copy(f"{name}D", self.to_sibling, self.from_sibling, sibling, ("d",), [f"{name}sib"])
            plan.task(f"{name}own", self.own_task, [f"{name}D"], time)
            ends = {1: (x_ahead, ("xF",)), 2: (x_across, ("xF", "xR")), 3: (x_back, ("xR",))}
            last = []
            for m in (1, 2, 3):
                if self.later and m == 2:
                    continue
                needs = [f"{name}rel"] if m == self.later else [f"{name}own"]
                last.append(f"{name}{m}")
                plan.copy(last[-1], self.sent.at[m - 1], self.arrived.at[m - 1], *ends[m], needs, 2 if m == 2 else 1)
            if self.later:
                plan.copy(f"{name}L", self.sent.at[1], self.relayed, *ends[self.later], [f"{name}own"])
                plan.task(f"{name}rel", self.relay_task, [f"{name}L", f"{name}own"], 0.1)
            return last

        def total(self):
            total = self.kept[...]
            for m in (1, 2, 3):
                if not (self.later and m == 2):
                    total = total + self.arrived[m - 1].astype(F32)
            return total

    def middle_task(s):
        full[1, 0, 0, s] = (full[0, 0, 0, s].astype(F32) + sums[0, s][0].total()).astype(BF16)

    def out_task(s):
        parts = [part.total() for part in sums[1, s]]
        if len(parts) > 1:
            parts = [part[:, 32 * i : 32 * i + 32] for i in range(4) for part in parts]
            parts = [jnp.concatenate(parts, axis=1)]
        result = full[1, 0, 0, s].astype(F32) + parts[0]
        out[LENGTH * s : LENGTH * s + LENGTH, :] = result.astype(BF16)

    def up_task(s):
        upward = jnp.maximum(product(normalised(1, s, mlp_gain), up), 0.0)
        hidden[s] = (upward * upward).astype(BF16)

    sums = {}
    for s in range(SEQS):
        plan.task(f"gate{s}", functools.partial(gate_task, s), complete["vg"] | set(gathered[0, s]), 0.35)
        plan.task(f"filter{s}", functools.partial(filter_task, s), [f"gate{s}"], 0.35)
        names = []
        for j in range(1, 8):
            names.append(f"t{s}{j}")
            peer = f"t{j}", {"tp": lax.rem(tp + j, 8)}
            plan.copy(names[-1], stats.at[s], stats_in.at[s, j - 1], peer, ("t",), [f"filter{s}"], 2)
        plan.task(f"act{s}", functools.partial(activate_task, s), names, 0.3)
        part = Sums(f"r0{s}", 0, s, activated, mx, 0, 64, X_SUM[0][s], wide)
        sums[0, s] = [part]
        plan.task(f"mid{s}", functools.partial(middle_task, s), part.plan(complete["mx"] | {f"act{s}"}, 0.25), 0.15)
        plan.task(f"up{s}", functools.partial(up_task, s), complete["up"] | set(gathered[1, s]), 0.5)
        sums[1, s], last = [], []
        for p, name in enumerate([name for name in WAYS if name in ("dn", "dm")]):
            way = WAYS[name]
            buffers = wide if way.high - way.low == 64 else narrow
            p = 1 if buffers is wide else p
            part = Sums(f"{name}{s}", p, s, hidden, dn, way.low, way.high, X_SUM[1][s], buffers)
            sums[1, s].append(part)
            last += part.plan(complete[name] | {f"up{s}"}, 0.5 if buffers is wide else 0.3)
        plan.task(f"out{s}", functools.partial(out_task, s), last, 0.15)
    plan.emit()


SEND_SEMS, RECEIVE_SEMS = 36, 93


def sum_buffers(width):
    shapes = [((4,), BF16), ((4,), BF16), ((), F32), ((3,), BF16), ((), F32), ((), BF16), ((3,), BF16)]
    return [pltpu.VMEM((2, SEQS, *lead, LENGTH, width), dtype) for lead, dtype in shapes]


def body(states, mix_gain, w_value, w_gate, conv_kernel, chan_gain, w_mix_out, mlp_gain, w_up, w_down_t):
    anywhere = pl.BlockSpec(memory_space=pltpu.HBM)
    vmem = pl.BlockSpec(memory_space=pltpu.VMEM)
    block = (LENGTH, 256)
    return pl.pallas_call(
        kernel,
        name="layer",
        out_shape=jax.ShapeDtypeStruct((SEQS * LENGTH, 256), BF16),
        in_specs=[anywhere] * 10,
        out_specs=vmem,
        scratch_shapes=[
            *[pltpu.VMEM((8, 4, 64, COLUMNS[name]), BF16) for name in ("vg", "mx", "up", "dn")],
            pltpu.VMEM((2, 2, 4, SEQS, *block), BF16),
            pltpu.VMEM((KWIDTH, 256), F32),
            pltpu.VMEM((1, 256), F32),
            pltpu.VMEM((2, SEQS, 160, 128), F32),
            pltpu.VMEM((SEQS, *block), F32),
            pltpu.VMEM((SEQS, 8, 128), F32),
            pltpu.VMEM((SEQS, 7, 8, 128), F32),
            pltpu.VMEM((SEQS, *block), BF16),
            pltpu.VMEM((SEQS, LENGTH, 768), BF16),
            pltpu.VMEM((1, D), F32),
            pltpu.VMEM((1, D), F32),
            pltpu.SemaphoreType.DMA((10,)),
            pltpu.SemaphoreType.DMA((SEND_SEMS,)),
            pltpu.SemaphoreType.DMA((RECEIVE_SEMS,)),
            *sum_buffers(256),
            *sum_buffers(128),
        ],
        compiler_params=pltpu.CompilerParams(
            collective_id=0, has_side_effects=True, vmem_limit_bytes=67043328
        ),
    )(
        states.reshape(SEQS, *block), w_value, w_gate, w_mix_out, w_up, w_down_t, conv_kernel,
        chan_gain.reshape(1, D), mix_gain.reshape(1, D), mlp_gain.reshape(1, D),
    )


def solution(mesh):
    return jax.shard_map(
        body,
        mesh=mesh,
        in_specs=(
            P(("rep", "fs"), "tp"),
            P(),
            P("fs", "tp"),
            P("fs", "tp"),
            P(),
            P(),
            P("fs", "tp"),
            P(),
            P("fs", "tp"),
            P("fs", "tp"),
        ),
        out_specs=P(("rep", "fs"), "tp"),
        check_vma=False,
    )
```

time: 94.7 us -> 84.4 us (0.89); the launches traced: 94.5 us -> 83.2 us
  Pallas kernels: 92.9 us -> 81.6 us
    pallas_call x1, Pallas kernels: 92.9 us -> 81.6 us  [body(): pl.pallas_call(kernel, name='layer', out_shape=jax.ShapeDtypeStruct((SEQS...]
where the time goes in v3:
time: 84.4 us; the launch traced here: 83.2 us
  Pallas kernels  81.6 us (97%)
  local copies, waits for them, and re-layouts  1.62 us (2%)
    pallas_call x1, Pallas kernels, body(): pl.pallas_call(kernel, name='layer', out_shape=jax.ShapeDtypeStruct((SEQS...  81.6 us

profile of v3, /device:TPU:1, one launch (start us, length us, event | category | flops | bytes accessed | tf_op | source)
XLA Modules:
  0.0 83.2 jit_solution(9067308737089029571)
XLA Ops:
  0.0 81.6 %layer.1 = bf16[384,256]{1,0:T(8,128)(2,1)} custom-call(bf16[3,128,256]{2,1,0:T(8,128)(2,1)} %bitcast.4, bf16[64,256]{1,0:T(8,128)(2,1)} %w_value.1, bf16[64,256]{1,0:T(8,128)(2,1)} %w_gate.1, bf16[64,256]{1,0:T(8,128)(2,1)} %w_mix.1, bf16[64,768]{1,0:T(8,128)(2,1)} %w_up.1, bf16[64,768]{1,0:T(8,128)(2,1)} %w_down.1, f32[31,2048]{1,0:T(8,128)} %conv.1, ...), custom_call_target="tpu_custom_call" | custom-call | tf_op jit(solution)/shard_map/layer/pallas_call | solution.py:478
  81.6 1.6 %copy.12 = bf16[384,256]{1,0:T(8,128)(2,1)} copy(bf16[384,256]{1,0:T(8,128)(2,1)} %layer.1) | data formatting | bytes 393216

commit v4 on v3

--- a/solution.py
+++ b/solution.py
@@ -28,17 +28,17 @@
 
 COLUMNS = {"vg": 512, "mx": 256, "up": 768, "dn": 768}
 WAYS = {
-    "vg": Way((0, 64), 32, EIGHT, "FRRFFRRF", "ring", "ring", "FFFRRR", True, (0, 1, 2, 3, 4), 2.0),
-    "mx": Way((0, 64), 40, FOUR, "FRRF", "ring", "ring", "FFFRRR", True, (0, 2, 4), 2.0),
-    "up": Way((0, 64), 48, EIGHT, "FRRFFRRF", "ring", "ring", "FRRFRF", False, (0, 2, 4), 0.0),
-    "dn": Way((0, 32), 16, FOUR, "FRRF", "ring", "ring", "FFRFRF", False, (0, 4), 2.0),
-    "dm": Way((32, 64), 16, FOUR, "FRRF", "ring", "ring", "FRRFFF", False, (0, 2, 4), -2.0),
+    "vg": Way((0, 64), 32, EIGHT, "FRRFFRRF", "three", "ring", "FFFFRR", True, (0, 1, 2, 3, 4), -1.9),
+    "mx": Way((0, 64), 48, FOUR, "FRRF", "ring", "ring", "FRFFRR", False, (0, 2, 4), -0.2),
+    "up": Way((0, 64), 48, EIGHT, "FRRFFRRF", "ring", "ring", "RRFRRF", False, (0, 2, 4), -0.8),
+    "dn": Way((0, 32), 16, FOUR, "FRRF", "three", "ring", "FRRRFR", False, (0, 4), 3.2),
+    "dm": Way((32, 64), 16, FOUR, "FRFF", "ring", "ring", "RRRFRR", False, (0, 2, 4), -4.2),
 }
-X_GATHER = ('RRD', 'DRD')
-X_SUM = ('RDD', 'DRF')
+X_GATHER = ('RRR', 'DRD')
+X_SUM = ('DDD', 'DRF')
 
 RATE = 46600.0
-SIBLING_RATE = 300000.0
+SIBLING_RATE = 500000.0
 HOP = 3.2
 FURTHER_HOP = 0.5
 SIBLING_HOP = 1.0
@@ -463,7 +463,7 @@
     plan.emit()
 
 
-SEND_SEMS, RECEIVE_SEMS = 36, 93
+SEND_SEMS, RECEIVE_SEMS = 36, 91
 
 
 def sum_buffers(width):

time: 84.4 us -> 84.1 us (level); the launches traced: 83.2 us -> 83.9 us
  no operation moved by 1% of the time
where the time goes in v4:
time: 84.1 us; the launch traced here: 83.9 us
  Pallas kernels  82.3 us (98%)
  local copies, waits for them, and re-layouts  1.62 us (2%)
    pallas_call x1, Pallas kernels, body(): pl.pallas_call(kernel, name='layer', out_shape=jax.ShapeDtypeStruct((SEQS...  82.3 us

profile of v4, /device:TPU:1, one launch (start us, length us, event | category | flops | bytes accessed | tf_op | source)
XLA Modules:
  0.0 83.9 jit_solution(16844644201421711836)
XLA Ops:
  0.0 82.3 %layer.1 = bf16[384,256]{1,0:T(8,128)(2,1)} custom-call(bf16[3,128,256]{2,1,0:T(8,128)(2,1)} %bitcast.4, bf16[64,256]{1,0:T(8,128)(2,1)} %w_value.1, bf16[64,256]{1,0:T(8,128)(2,1)} %w_gate.1, bf16[64,256]{1,0:T(8,128)(2,1)} %w_mix.1, bf16[64,768]{1,0:T(8,128)(2,1)} %w_up.1, bf16[64,768]{1,0:T(8,128)(2,1)} %w_down.1, f32[31,2048]{1,0:T(8,128)} %conv.1, ...), custom_call_target="tpu_custom_call" | custom-call | tf_op jit(solution)/shard_map/layer/pallas_call | solution.py:478
  82.3 1.6 %copy.12 = bf16[384,256]{1,0:T(8,128)(2,1)} copy(bf16[384,256]{1,0:T(8,128)(2,1)} %layer.1) | data formatting | bytes 393216

commit v5 on v4

--- a/solution.py
+++ b/solution.py
@@ -39,7 +39,7 @@
 
 RATE = 46600.0
 SIBLING_RATE = 500000.0
-HOP = 3.2
+HOP = 3.35
 FURTHER_HOP = 0.5
 SIBLING_HOP = 1.0
 PER_COPY = 0.08
@@ -439,18 +439,18 @@
 
     sums = {}
     for s in range(SEQS):
-        plan.task(f"gate{s}", functools.partial(gate_task, s), complete["vg"] | set(gathered[0, s]), 0.35)
-        plan.task(f"filter{s}", functools.partial(filter_task, s), [f"gate{s}"], 0.35)
+        plan.task(f"gate{s}", functools.partial(gate_task, s), complete["vg"] | set(gathered[0, s]), 0.3)
+        plan.task(f"filter{s}", functools.partial(filter_task, s), [f"gate{s}"], 0.33)
         names = []
         for j in range(1, 8):
             names.append(f"t{s}{j}")
             peer = f"t{j}", {"tp": lax.rem(tp + j, 8)}
             plan.copy(names[-1], stats.at[s], stats_in.at[s, j - 1], peer, ("t",), [f"filter{s}"], 2)
-        plan.task(f"act{s}", functools.partial(activate_task, s), names, 0.3)
+        plan.task(f"act{s}", functools.partial(activate_task, s), names, 0.2)
         part = Sums(f"r0{s}", 0, s, activated, mx, 0, 64, X_SUM[0][s], wide)
         sums[0, s] = [part]
-        plan.task(f"mid{s}", functools.partial(middle_task, s), part.plan(complete["mx"] | {f"act{s}"}, 0.25), 0.15)
-        plan.task(f"up{s}", functools.partial(up_task, s), complete["up"] | set(gathered[1, s]), 0.5)
+        plan.task(f"mid{s}", functools.partial(middle_task, s), part.plan(complete["mx"] | {f"act{s}"}, 0.15), 0.15)
+        plan.task(f"up{s}", functools.partial(up_task, s), complete["up"] | set(gathered[1, s]), 0.45)
         sums[1, s], last = [], []
         for p, name in enumerate([name for name in WAYS if name in ("dn", "dm")]):
             way = WAYS[name]
@@ -458,12 +458,12 @@
             p = 1 if buffers is wide else p
             part = Sums(f"{name}{s}", p, s, hidden, dn, way.low, way.high, X_SUM[1][s], buffers)
             sums[1, s].append(part)
-            last += part.plan(complete[name] | {f"up{s}"}, 0.5 if buffers is wide else 0.3)
+            last += part.plan(complete[name] | {f"up{s}"}, 0.4 if buffers is wide else 0.2)
         plan.task(f"out{s}", functools.partial(out_task, s), last, 0.15)
     plan.emit()
 
 
-SEND_SEMS, RECEIVE_SEMS = 36, 91
+SEND_SEMS, RECEIVE_SEMS = 36, 92
 
 
 def sum_buffers(width):

time: 84.1 us -> 83.3 us (level)
  no operation moved by 1% of the time
where the time goes in v5:
time: 83.3 us; the launch traced here: 83.1 us
  Pallas kernels  81.5 us (98%)
  local copies, waits for them, and re-layouts  1.62 us (2%)
    pallas_call x1, Pallas kernels, body(): pl.pallas_call(kernel, name='layer', out_shape=jax.ShapeDtypeStruct((SEQS...  81.5 us

profile of v5, /device:TPU:1, one launch (start us, length us, event | category | flops | bytes accessed | tf_op | source)
XLA Modules:
  0.0 83.1 jit_solution(5367248766705019235)
XLA Ops:
  0.0 81.5 %layer.1 = bf16[384,256]{1,0:T(8,128)(2,1)} custom-call(bf16[3,128,256]{2,1,0:T(8,128)(2,1)} %bitcast.4, bf16[64,256]{1,0:T(8,128)(2,1)} %w_value.1, bf16[64,256]{1,0:T(8,128)(2,1)} %w_gate.1, bf16[64,256]{1,0:T(8,128)(2,1)} %w_mix.1, bf16[64,768]{1,0:T(8,128)(2,1)} %w_up.1, bf16[64,768]{1,0:T(8,128)(2,1)} %w_down.1, f32[31,2048]{1,0:T(8,128)} %conv.1, ...), custom_call_target="tpu_custom_call" | custom-call | tf_op jit(solution)/shard_map/layer/pallas_call | solution.py:478
  81.5 1.6 %copy.12 = bf16[384,256]{1,0:T(8,128)(2,1)} copy(bf16[384,256]{1,0:T(8,128)(2,1)} %layer.1) | data formatting | bytes 393216
